TPU v7x, 512 devices: a whole 4x4x16 slice. The times are simulated.
512 devices in a mesh: sp: 128 (over z, x, core), tp: 4 (over y).
Axes of the slice: x: 4, y: 4, z: 16, core: 2. Of those that a mesh axis runs over, the one named last changes fastest.
Arguments:
- hidden_in: bfloat16 [32768, 2048], P('sp'), may hold values from -8 to 8
- w_convb: bfloat16 [2048, 1024], P('sp', 'tp'), may hold values from -0.125 to 0.125
- w_convc: bfloat16 [2048, 1024], P('sp', 'tp'), may hold values from -0.125 to 0.125
- w_convx: bfloat16 [2048, 1024], P('sp', 'tp'), may hold values from -0.125 to 0.125
- w_query: bfloat16 [2048, 1024], P('sp', 'tp'), may hold values from -1 to 1
- w_key: bfloat16 [2048, 1024], P('sp', 'tp'), may hold values from -1 to 1
- w_value: bfloat16 [2048, 1024], P('sp', 'tp'), may hold values from -0.125 to 0.125
- conv_taps: float32 [3, 1024], P(None, 'tp'), may hold values from -3.5 to 3.5
- gate_cache: float32 [32768, 16], P(None, 'tp'), as said below
- w_out_conv: bfloat16 [1024, 2048], P('tp'), may hold values from -0.125 to 0.125
- w_out_attn: bfloat16 [1024, 2048], P('tp'), may hold values from -0.125 to 0.125
Outputs:
- mixed: bfloat16 [32768, 2048], P(('sp', 'tp'))
Inputs may be any that keep to these rules, and one draw needn't show every extreme that they name: `gate_cache`: down each column, read from row 4096 to the last row and then from row 0 on, the values never rise.
All inputs are finite; a program needn't handle non-finite values.
Results may differ from a plain program's by a relative error of at most 0.018.
Values may be sent and summed in bfloat16 or wider, within the bound.
No kernel may reach another device: no remote copies, remote signals or barrier semaphores. Data moves between devices by JAX's collectives and lax.ppermute only.
A program may use at most 128 MiB of HBM per device.

v0:
```python
import jax
import jax.numpy as jnp
from jax import lax
from jax.sharding import PartitionSpec as P

neg_large = -1e30


def sent_together(arrays, axis, dim, along):
    both = jnp.concatenate(arrays, axis=along)
    result, at, done = (lax.all_gather(both, axis, axis=dim, tiled=True), 0, [])
    for a in arrays:
        done.append(lax.slice_in_dim(result, at, at + a.shape[along], axis=along))
        at += a.shape[along]
    return tuple(done)


def shortened(shard):

    def short(part):
        return part.astype(jnp.bfloat16) if part.dtype == jnp.float32 else part

    return jax.tree.map(short, shard)


def passed_along(value, axis, steps):
    count = lax.axis_size(axis)
    pairs = [(source, (source + steps) % count) for source in range(count)]
    return lax.ppermute(value, axis, pairs)


def cut_along(shard, dim, size):
    before, after = (shard.shape[:dim], shard.shape[dim + 1 :])
    return jnp.moveaxis(shard.reshape(*before, size, -1, *after), dim, 0)


def sum_at_owner(shard, axis, dim):
    size = lax.axis_size(axis)
    blocks = lax.all_to_all(cut_along(shard, dim, size), axis, 0, 0, tiled=True)
    return jnp.sum(blocks.astype(jnp.float32), axis=0)


def project(weight_rows, hidden_in):
    return jnp.dot(hidden_in, weight_rows, preferred_element_type=jnp.float32)


def absorb(attn_state, query_heads, gate_rows, key_heads, value_heads, gate_cols, allowed):
    running_max, row_total, weighted = attn_state
    score_scale = query_heads.shape[2] ** (-0.5)
    scores = (
        jnp.einsum("qhd,khd->hqk", query_heads, key_heads, preferred_element_type=jnp.float32)
        * score_scale
    )
    scores = scores + gate_rows.T[:, :, None] - gate_cols.T[:, None, :]
    if allowed is not None:
        scores = jnp.where(allowed[None], scores, neg_large)
    new_max = jnp.maximum(running_max, jnp.max(scores, axis=2))
    weights = jnp.exp(scores - new_max[:, :, None])
    factor = jnp.exp(running_max - new_max)
    row_total = row_total * factor + jnp.sum(weights, axis=2)
    weighted = weighted * factor[:, :, None] + jnp.einsum(
        "hqk,khd->hqd",
        weights.astype(jnp.bfloat16),
        value_heads,
        preferred_element_type=jnp.float32,
    )
    return (new_max, row_total, weighted)


def shards(
    hidden_in,
    w_convb,
    w_convc,
    w_convx,
    w_query,
    w_key,
    w_value,
    conv_taps,
    gate_cache,
    w_out_conv,
    w_out_attn,
):
    tok_rows = hidden_in.shape[0]
    head_count = gate_cache.shape[1]
    attn_width = w_query.shape[1]
    head_depth = attn_width // head_count
    axis_length = lax.axis_size("sp")
    group_span = axis_length // 4
    seq_index = lax.axis_index("sp")
    position = (seq_index - group_span // 2) % group_span
    pieces = sent_together((w_convb, w_convc, w_convx, w_query, w_key, w_value), "sp", 0, 1)
    projected = tuple((project(weight_rows, hidden_in) for weight_rows in pieces))
    gate_b, gate_c, conv_values, query, keys, values = [
        partial_total.astype(jnp.bfloat16) for partial_total in projected
    ]
    conv_input = (gate_c.astype(jnp.float32) * conv_values.astype(jnp.float32)).astype(jnp.bfloat16)
    last_rows = conv_input[tok_rows - 2 :]
    query_heads = query.reshape(tok_rows, head_count, head_depth)
    key_heads = keys.reshape(tok_rows, head_count, head_depth)
    value_heads = values.reshape(tok_rows, head_count, head_depth)
    gate_rows = lax.dynamic_slice_in_dim(gate_cache, seq_index * tok_rows, tok_rows, 0)

    def gates_back(distance):
        source = (seq_index - distance + axis_length) % axis_length
        return lax.dynamic_slice_in_dim(gate_cache, source * tok_rows, tok_rows, 0)

    row_ids = jnp.arange(tok_rows, dtype=jnp.int32)
    allowed = row_ids[None, :] <= row_ids[:, None]
    initial = (
        jnp.full((head_count, tok_rows), neg_large, jnp.float32),
        jnp.zeros((head_count, tok_rows), jnp.float32),
        jnp.zeros((head_count, tok_rows, head_depth), jnp.float32),
    )
    attn_state = absorb(initial, query_heads, gate_rows, key_heads, value_heads, gate_rows, allowed)
    edge_rows = last_rows
    collected = (key_heads[None], value_heads[None])
    held_count = 1
    for doubling_level in range(group_span.bit_length() - 1):
        with_edge = held_count == 1
        payload = collected + (last_rows,) if with_edge else collected
        moved = jax.tree.map(
            lambda part, own: part.astype(own.dtype),
            passed_along(shortened(payload), "sp", held_count),
            payload,
        )
        if with_edge:
            edge_rows = moved[2]
        collected = (
            jnp.concatenate([moved[0], collected[0]], axis=0),
            jnp.concatenate([moved[1], collected[1]], axis=0),
        )
        held_count = held_count * 2

    def absorb_shard(shard_index, present_memory):
        distance = held_count - 1 - shard_index
        shard_keys = lax.dynamic_index_in_dim(collected[0], shard_index, 0, False)
        shard_values = lax.dynamic_index_in_dim(collected[1], shard_index, 0, False)
        source_gates = gates_back(distance)
        return lax.cond(
            distance <= position,
            lambda present: absorb(
                present, query_heads, gate_rows, shard_keys, shard_values, source_gates, None
            ),
            lambda present: present,
            present_memory,
        )

    attn_state = lax.fori_loop(0, held_count - 1, absorb_shard, attn_state)
    edge_rows = jnp.where(position > 0, edge_rows, jnp.zeros_like(edge_rows))
    padded = lax.optimization_barrier(jnp.concatenate([edge_rows, conv_input], axis=0)).astype(
        jnp.float32
    )
    mixed_conv = (
        conv_taps[0] * padded[:tok_rows]
        + conv_taps[1] * padded[1 : tok_rows + 1]
        + conv_taps[2] * padded[2:]
    )
    conv_out = (gate_b.astype(jnp.float32) * mixed_conv).astype(jnp.bfloat16)
    running_max, row_total, weighted = attn_state
    attn_out = (
        (weighted / row_total[:, :, None])
        .transpose(1, 0, 2)
        .reshape(tok_rows, attn_width)
        .astype(jnp.bfloat16)
    )
    mixed = sum_at_owner(
        (
            jnp.dot(conv_out, w_out_conv, preferred_element_type=jnp.float32)
            + jnp.dot(attn_out, w_out_attn, preferred_element_type=jnp.float32)
        ).astype(jnp.bfloat16),
        "tp",
        0,
    )
    return mixed.astype(jnp.bfloat16)


def solution(mesh):
    return jax.shard_map(
        shards,
        mesh=mesh,
        in_specs=(
            P("sp", None),
            P("sp", "tp"),
            P("sp", "tp"),
            P("sp", "tp"),
            P("sp", "tp"),
            P("sp", "tp"),
            P("sp", "tp"),
            P(None, "tp"),
            P(None, "tp"),
            P("tp", None),
            P("tp", None),
        ),
        out_specs=P(("sp", "tp"), None),
        check_vma=False,
    )
```

profile of v0, /device:TPU:38, one launch (start us, length us, event | category | flops | bytes accessed | tf_op | source)
XLA Modules:
  0.0 570.6 jit_solution(2518392395867211811)
XLA Ops:
  11.5 146.6 %all-gather.2.cloned.1.call-done = bf16[2048,1536]{1,0:T(8,128)(2,1)} async-done(((bf16[16,1536]{1,0:T(8,128)(2,1)}), bf16[2048,1536]{1,0:T(8,128)(2,1)}) %all-gather.2.cloned.1.call-update) | async-done | bytes 6291472 | tf_op jit(solution)/shard_map/all_gather | solution.py:11
  166.1 6.5 %collective-permute-start.2 = (bf16[2,256,4,64]{1,3,2,0:T(8,128)(2,1)S(1)}, bf16[2,256,4,64]{1,3,2,0:T(8,128)(2,1)S(1)}, u32[]{:S(2)}, u32[]{:S(2)}) collective-permute-start(bf16[2,256,4,64]{1,3,2,0:T(8,128)(2,1)S(1)} %pad_maximum_fusion.4), channel_id=1, source_target_pairs={{0,8},{4,12},{8,16},{12,20},{16,24},{20,28},{24,32},{28,36},{32,40... | collective-permute-start | bytes 786440 | tf_op jit(solution)/shard_map/ppermute | solution.py:29
  176.6 4.5 collective-permute-start.3
  181.9 3.9 collective-permute-start.7
  187.4 6.3 %collective-permute-done.3 = bf16[4,256,4,64]{1,3,2,0:T(8,128)(2,1)S(1)} collective-permute-done((bf16[4,256,4,64]{1,3,2,0:T(8,128)(2,1)S(1)}, bf16[4,256,4,64]{1,3,2,0:T(8,128)(2,1)S(1)}, u32[]{:S(2)}, u32[]{:S(2)}) %collective-permute-start.3) | collective-permute-done | bytes 524320 | tf_op jit(solution)/shard_map/ppermute | solution.py:29
  193.9 3.6 collective-permute-start.4
  199.2 5.5 collective-permute-start.8
  210.1 20.7 %collective-permute-done.8 = bf16[4,256,4,64]{1,3,2,0:T(8,128)(2,1)S(1)} collective-permute-done((bf16[4,256,4,64]{1,3,2,0:T(8,128)(2,1)S(1)}, bf16[4,256,4,64]{1,3,2,0:T(8,128)(2,1)S(1)}, u32[]{:S(2)}, u32[]{:S(2)}) %collective-permute-start.8) | collective-permute-done | bytes 524320 | tf_op jit(solution)/shard_map/ppermute | solution.py:29
  231.0 3.6 collective-permute-start.9
  242.6 18.4 %collective-permute-done.9 = bf16[8,256,4,64]{1,3,2,0:T(8,128)(2,1)S(1)} collective-permute-done((bf16[8,256,4,64]{1,3,2,0:T(8,128)(2,1)S(1)}, bf16[8,256,4,64]{1,3,2,0:T(8,128)(2,1)S(1)}, u32[]{:S(2)}, u32[]{:S(2)}) %collective-permute-start.9) | collective-permute-done | bytes 1048608 | tf_op jit(solution)/shard_map/ppermute | solution.py:29
  265.1 4.2 collective-permute-start.10
  273.7 58.3 %collective-permute-done.5 = bf16[16,256,4,64]{1,3,2,0:T(8,128)(2,1)} collective-permute-done((bf16[16,256,4,64]{1,3,2,0:T(8,128)(2,1)}, bf16[16,256,4,64]{1,3,2,0:T(8,128)(2,1)}, u32[]{:S(2)}, u32[]{:S(2)}) %collective-permute-start.5) | collective-permute-done | bytes 2097184 | tf_op jit(solution)/shard_map/ppermute | solution.py:29
  334.1 101.6 %collective-permute-done.10 = bf16[16,256,4,64]{1,3,2,0:T(8,128)(2,1)} collective-permute-done((bf16[16,256,4,64]{1,3,2,0:T(8,128)(2,1)}, bf16[16,256,4,64]{1,3,2,0:T(8,128)(2,1)}, u32[]{:S(2)}, u32[]{:S(2)}) %collective-permute-start.10) | collective-permute-done | bytes 2097184 | tf_op jit(solution)/shard_map/ppermute | solution.py:29
  439.8 106.4 %while.19 = (s32[]{:T(128)}, f32[4,256]{1,0:T(4,128)S(1)}, f32[4,256]{1,0:T(4,128)S(1)}, f32[4,256,64]{1,2,0:T(8,128)S(1)}, s32[]{:T(128)}, /*index=5*/s32[]{:T(...) while((s32[]{:T(128)}, f32[4,256]{1,0:T(4,128)S(1)}, ...), condition=%wide.region_7.8_spmd, body=%wide.region_2.7_spmd.sunk | while | flops 69339152 | bytes 4145680 | solution.py:148
  457.5 3.5 conditional.2
  468.1 3.5 conditional.2
  478.8 3.5 conditional.2
  489.4 3.5 conditional.2
  500.0 3.5 conditional.2
  510.7 3.5 conditional.2
  521.3 3.5 conditional.2
  532.0 3.5 conditional.2
  542.6 3.5 conditional.2
  547.9 15.0 %all_to_all.5 = bf16[4,64,2048]{2,1,0:T(8,128)(2,1)S(1)} all-to-all(bf16[4,64,2048]{2,1,0:T(8,128)(2,1)S(1)} %bitcast.70), channel_id=1, replica_groups=mesh['sp'=128,'tp'=4] {'tp'}, dimensions={0} | all-to-all | bytes 2097152 | tf_op jit(solution)/shard_map/all_to_all | solution.py:39
  (350 shorter events, 228.5 us)
Async XLA Ops:
  6.5 151.5 %copy-start = (bf16[256,2048]{1,0:T(8,128)(2,1)S(1)}, bf16[256,2048]{1,0:T(8,128)(2,1)}, u32[]{:S(2)}) copy-start(bf16[256,2048]{1,0:T(8,128)(2,1)} %param.15) | copy-start | bytes 3145732
  6.5 151.5 %all-gather.2.cloned.1.call-start = ((), (), s32[]{:S(2)}) async-start(), calls=%async_computation.1 | async-start | bytes 6340608 | tf_op jit(solution)/shard_map/all_gather | solution.py:11
  159.8 78.7 %copy-start.14 = (bf16[256,256]{1,0:T(8,128)(2,1)}, bf16[256,256]{1,0:T(8,128)(2,1)S(1)}, u32[]{:S(2)}) copy-start(bf16[256,256]{1,0:T(8,128)(2,1)S(1)} %convolution_convert_fusion.4) | copy-start | bytes 393220
  159.8 6.3 %collective-permute-start.1 = (bf16[1,256,4,64]{1,3,2,0:T(8,128)(2,1)S(1)}, bf16[1,256,4,64]{1,3,2,0:T(8,128)(2,1)S(1)}, u32[]{:S(2)}, u32[]{:S(2)}) collective-permute-start(bf16[1,256,4,64]{1,3,2,0:T(8,128)(2,1)S(1)} %bitcast.73), channel_id=1, source_target_pairs={{0,4},{4,8},{8,12},{12,16},{16,20},{20,24},{24,28},{28,32},{32,36}... | collective-permute-start | bytes 393224 | tf_op jit(solution)/shard_map/ppermute | solution.py:29
  166.1 10.4 %collective-permute-start.2 = (bf16[2,256,4,64]{1,3,2,0:T(8,128)(2,1)S(1)}, bf16[2,256,4,64]{1,3,2,0:T(8,128)(2,1)S(1)}, u32[]{:S(2)}, u32[]{:S(2)}) collective-permute-start(bf16[2,256,4,64]{1,3,2,0:T(8,128)(2,1)S(1)} %pad_maximum_fusion.4), channel_id=1, source_target_pairs={{0,8},{4,12},{8,16},{12,20},{16,24},{20,28},{24,32},{28,36},{32,40... | collective-permute-start | bytes 786440 | tf_op jit(solution)/shard_map/ppermute | solution.py:29
  174.3 7.5 %collective-permute-start.6 = (bf16[1,256,4,64]{1,3,2,0:T(8,128)(2,1)S(1)}, bf16[1,256,4,64]{1,3,2,0:T(8,128)(2,1)S(1)}, u32[]{:S(2)}, u32[]{:S(2)}) collective-permute-start(bf16[1,256,4,64]{1,3,2,0:T(8,128)(2,1)S(1)} %bitcast.63), channel_id=1, source_target_pairs={{0,4},{4,8},{8,12},{12,16},{16,20},{20,24},{24,28},{28,32},{32,36}... | collective-permute-start | bytes 393224 | tf_op jit(solution)/shard_map/ppermute | solution.py:29
  176.5 60.5 %copy-start.9 = (bf16[2,256,4,64]{1,3,2,0:T(8,128)(2,1)}, bf16[2,256,4,64]{1,3,2,0:T(8,128)(2,1)S(1)}, u32[]{:S(2)}) copy-start(bf16[2,256,4,64]{1,3,2,0:T(8,128)(2,1)S(1)} %collective-permute-done.2) | copy-start | bytes 786436
  176.6 17.1 %collective-permute-start.3 = (bf16[4,256,4,64]{1,3,2,0:T(8,128)(2,1)S(1)}, bf16[4,256,4,64]{1,3,2,0:T(8,128)(2,1)S(1)}, u32[]{:S(2)}, u32[]{:S(2)}) collective-permute-start(bf16[4,256,4,64]{1,3,2,0:T(8,128)(2,1)S(1)} %pad_maximum_fusion.2), channel_id=1, source_target_pairs={{0,16},{4,20},{8,24},{12,28},{16,32},{20,36},{24,40},{28,44},{32,4... | collective-permute-start | bytes 1572872 | tf_op jit(solution)/shard_map/ppermute | solution.py:29
  181.9 17.3 %collective-permute-start.7 = (bf16[2,256,4,64]{1,3,2,0:T(8,128)(2,1)S(1)}, bf16[2,256,4,64]{1,3,2,0:T(8,128)(2,1)S(1)}, u32[]{:S(2)}, u32[]{:S(2)}) collective-permute-start(bf16[2,256,4,64]{1,3,2,0:T(8,128)(2,1)S(1)} %pad_maximum_fusion.5), channel_id=1, source_target_pairs={{0,8},{4,12},{8,16},{12,20},{16,24},{20,28},{24,32},{28,36},{32,40... | collective-permute-start | bytes 786440 | tf_op jit(solution)/shard_map/ppermute | solution.py:29
  193.9 41.2 %collective-permute-start.4 = (bf16[8,256,4,64]{1,3,2,0:T(8,128)(2,1)S(1)}, bf16[8,256,4,64]{1,3,2,0:T(8,128)(2,1)S(1)}, u32[]{:S(2)}, u32[]{:S(2)}) collective-permute-start(bf16[8,256,4,64]{1,3,2,0:T(8,128)(2,1)S(1)} %pad_maximum_fusion), channel_id=1, source_target_pairs={{0,32},{4,36},{8,40},{12,44},{16,48},{20,52},{24,56},{28,60},{32,6... | collective-permute-start | bytes 3145736 | tf_op jit(solution)/shard_map/ppermute | solution.py:29
  199.1 63.9 %copy-start.11 = (bf16[2,256,4,64]{1,3,2,0:T(8,128)(2,1)}, bf16[2,256,4,64]{1,3,2,0:T(8,128)(2,1)S(1)}, u32[]{:S(2)}) copy-start(bf16[2,256,4,64]{1,3,2,0:T(8,128)(2,1)S(1)} %collective-permute-done.7) | copy-start | bytes 786436
  199.2 31.6 %collective-permute-start.8 = (bf16[4,256,4,64]{1,3,2,0:T(8,128)(2,1)S(1)}, bf16[4,256,4,64]{1,3,2,0:T(8,128)(2,1)S(1)}, u32[]{:S(2)}, u32[]{:S(2)}) collective-permute-start(bf16[4,256,4,64]{1,3,2,0:T(8,128)(2,1)S(1)} %pad_maximum_fusion.3), channel_id=1, source_target_pairs={{0,16},{4,20},{8,24},{12,28},{16,32},{20,36},{24,40},{28,44},{32,4... | collective-permute-start | bytes 1572872 | tf_op jit(solution)/shard_map/ppermute | solution.py:29
  206.4 63.3 %collective-permute-start = (bf16[2,256]{1,0:T(2,128)(2,1)S(1)}, bf16[2,256]{1,0:T(2,128)(2,1)S(1)}, u32[]{:S(2)}, u32[]{:S(2)}) collective-permute-start(bf16[2,256]{1,0:T(2,128)(2,1)S(1)} %slice.55), channel_id=1, source_target_pairs={{0,4},{4,8},{8,12},{12,16},{16,20},{20,24},{24,28},{28,32},{32,36}... | collective-permute-start | bytes 3080 | tf_op jit(solution)/shard_map/ppermute | solution.py:29
  231.0 30.0 %collective-permute-start.9 = (bf16[8,256,4,64]{1,3,2,0:T(8,128)(2,1)S(1)}, bf16[8,256,4,64]{1,3,2,0:T(8,128)(2,1)S(1)}, u32[]{:S(2)}, u32[]{:S(2)}) collective-permute-start(bf16[8,256,4,64]{1,3,2,0:T(8,128)(2,1)S(1)} %pad_maximum_fusion.1), channel_id=1, source_target_pairs={{0,32},{4,36},{8,40},{12,44},{16,48},{20,52},{24,56},{28,60},{32,6... | collective-permute-start | bytes 3145736 | tf_op jit(solution)/shard_map/ppermute | solution.py:29
  239.1 93.0 %collective-permute-start.5 = (bf16[16,256,4,64]{1,3,2,0:T(8,128)(2,1)}, bf16[16,256,4,64]{1,3,2,0:T(8,128)(2,1)}, u32[]{:S(2)}, u32[]{:S(2)}) collective-permute-start(bf16[16,256,4,64]{1,3,2,0:T(8,128)(2,1)} %constant_dynamic-update-slice_fusion.6), channel_id=1, source_target_pairs={{0,64},{4,68},{8,72},{12,76},{16,80},{20,84},{24,88},{28,92},{32,9... | collective-permute-start | bytes 6291464 | tf_op jit(solution)/shard_map/ppermute | solution.py:29
  265.1 170.7 %collective-permute-start.10 = (bf16[16,256,4,64]{1,3,2,0:T(8,128)(2,1)}, bf16[16,256,4,64]{1,3,2,0:T(8,128)(2,1)}, u32[]{:S(2)}, u32[]{:S(2)}) collective-permute-start(bf16[16,256,4,64]{1,3,2,0:T(8,128)(2,1)} %constant_dynamic-update-slice_fusion.17), channel_id=1, source_target_pairs={{0,64},{4,68},{8,72},{12,76},{16,80},{20,84},{24,88},{28,92},{32,9... | collective-permute-start | bytes 6291464 | tf_op jit(solution)/shard_map/ppermute | solution.py:29
  273.7 60.3 %copy-start.10 = (bf16[2,256,4,64]{1,3,2,0:T(8,128)(2,1)S(1)}, bf16[2,256,4,64]{1,3,2,0:T(8,128)(2,1)}, u32[]{:S(2)}) copy-start(bf16[2,256,4,64]{1,3,2,0:T(8,128)(2,1)} %copy-done.9) | copy-start | bytes 786436
  273.7 60.4 %copy-start.18 = (bf16[1,256,4,64]{1,3,2,0:T(8,128)(2,1)S(1)}, bf16[1,256,4,64]{1,3,2,0:T(8,128)(2,1)}, u32[]{:S(2)}) copy-start(bf16[1,256,4,64]{1,3,2,0:T(8,128)(2,1)} %copy-done.16) | copy-start | bytes 393220
  273.7 60.4 %copy-start.15 = (bf16[256,256]{1,0:T(8,128)(2,1)S(1)}, bf16[256,256]{1,0:T(8,128)(2,1)}, u32[]{:S(2)}) copy-start(bf16[256,256]{1,0:T(8,128)(2,1)} %copy-done.14) | copy-start | bytes 393220
  333.8 103.7 %copy-start.8 = (bf16[8,256,4,64]{1,3,2,0:T(8,128)(2,1)S(1)}, bf16[8,256,4,64]{1,3,2,0:T(8,128)(2,1)}, u32[]{:S(2)}) copy-start(bf16[8,256,4,64]{1,3,2,0:T(8,128)(2,1)} %copy-done.7) | copy-start | bytes 3145732
  333.9 103.7 %copy-start.4 = (bf16[4,256,4,64]{1,3,2,0:T(8,128)(2,1)S(1)}, bf16[4,256,4,64]{1,3,2,0:T(8,128)(2,1)}, u32[]{:S(2)}) copy-start(bf16[4,256,4,64]{1,3,2,0:T(8,128)(2,1)} %copy-done.3) | copy-start | bytes 1572868
  334.0 103.7 %copy-start.12 = (bf16[2,256,4,64]{1,3,2,0:T(8,128)(2,1)S(1)}, bf16[2,256,4,64]{1,3,2,0:T(8,128)(2,1)}, u32[]{:S(2)}) copy-start(bf16[2,256,4,64]{1,3,2,0:T(8,128)(2,1)} %copy-done.11) | copy-start | bytes 786436
  334.0 103.6 %copy-start.21 = (bf16[1,256,4,64]{1,3,2,0:T(8,128)(2,1)S(1)}, bf16[1,256,4,64]{1,3,2,0:T(8,128)(2,1)}, u32[]{:S(2)}) copy-start(bf16[1,256,4,64]{1,3,2,0:T(8,128)(2,1)} %copy-done.19) | copy-start | bytes 393220
  334.1 103.6 %copy-start.22 = (bf16[32,256,4,64]{1,3,2,0:T(8,128)(2,1)}, bf16[32,256,4,64]{1,3,2,0:T(8,128)(2,1)S(1)}, u32[]{:S(2)}) copy-start(bf16[32,256,4,64]{1,3,2,0:T(8,128)(2,1)S(1)} %constant_dynamic-update-slice_fusion.11) | copy-start | bytes 12582916
  (13 other events, 421.7 us)
Sparse Core Ops, SparseCore 0:
  11.6 146.4 all-gather.1
where the time goes:
time: 574 us; the launch traced here: 571 us
  waiting for transfers between devices  356 us (62%)
  matrix products  90.9 us (16%)
  local copies, waits for them, and re-layouts  42.5 us (7%)
  starting transfers between devices  41.3 us (7%)
  blocking collectives  15 us (3%)
  between operations  14 us (2%)
  other arithmetic  7.91 us (1%)
    ppermute x11, waiting for transfers between devices, passed_along(): return lax.ppermute(value, axis, pairs)  209 us
    all_gather x1, waiting for transfers between devices, sent_together(): result, at, done = (lax.all_gather(both, axis, axis=dim, tiled=True), 0, [])  147 us
    ppermute x11, starting transfers between devices, passed_along(): return lax.ppermute(value, axis, pairs)  41.3 us
    dot_general x31, matrix products, absorb(): jnp.einsum('qhd,khd->hqk', query_heads, key_heads, preferred_element_type...  40.7 us
    dot_general x31, matrix products, absorb(): jnp.einsum('hqk,khd->hqd', weights.astype(jnp.bfloat16), value_heads, pre...  37 us
    transpose x31, local copies, waits for them, and re-layouts, absorb(): scores = scores + gate_rows.T[:, :, None] - gate_cols.T[:, None, :]  21.5 us
    unnamed x73, local copies, waits for them, and re-layouts  16.8 us
    all_to_all x1, blocking collectives, sum_at_owner(): blocks = lax.all_to_all(cut_along(shard, dim, size), axis, 0, 0, tiled=True)  15 us
  transfers between devices with their start and end apart: 12, of which 9 were waited for; matrix products, arithmetic and copies ran while one was open for 4% of the time, Pallas kernels for 0%

commit v1 on v0

v1 whole, which is shorter than its diff:
```python
import functools

import jax
import jax.numpy as jnp
from jax import lax
from jax.experimental import pallas as pl
from jax.experimental.pallas import tpu as pltpu
from jax.sharding import Mesh, PartitionSpec as P

LOG2E = 1.4426950408889634
NEG = -1e30
BLK = 256
bf16 = jnp.bfloat16
f32 = jnp.float32


def dot_t(a, b):
    return lax.dot_general(a, b, (((0,), (0,)), ((), ())), preferred_element_type=f32)


def attend_kernel(where, kv, q, gate, *refs, last):
    if last:
        acc_in, ml_in, out, kbuf, qbuf, acc, ml = refs
    else:
        acc, ml, kbuf, qbuf = refs
    core = where[0]
    xi = where[1]
    hd = kv.shape[3]
    aug = kbuf.shape[2]
    cb = 1 - core if last else core

    if last:
        acc[...] = acc_in[...]
        ml[...] = ml_in[...]
    else:
        acc[...] = jnp.zeros_like(acc)
        line = lax.broadcasted_iota(jnp.int32, ml.shape, 1)
        ml[...] = jnp.where(line == 0, NEG, 0.0)

    row = lax.broadcasted_iota(jnp.int32, (aug - hd, BLK), 0)
    ones = jnp.where(row < 3, 1.0, 0.0).astype(bf16)
    for j in range(4):
        qbuf[j, 0:hd, :] = q[j]
        qbuf[j, hd:aug, :] = ones
    first = gate[0:1, 0:1]
    for z in range(4):
        for x in range(4):
            b = (first - gate[pl.ds(z * 8 + x * 2 + cb, 1), :]) * LOG2E
            hi = b.astype(bf16).astype(f32)
            rest = b - hi
            mid = rest.astype(bf16).astype(f32)
            lo = rest - mid
            rows = jnp.where(row == 0, hi, jnp.where(row == 1, mid, jnp.where(row == 2, lo, 0.0)))
            kbuf[x, z, 0:hd, :] = kv[x, z, 0]
            kbuf[x, z, hd:aug, :] = rows.astype(bf16)

    def step(j, blocks, allowed=None):
        m = ml[j, 0:1, :]
        qj = qbuf[j]
        ss = [dot_t(kbuf[x, z], qj) for x, z in blocks]
        if allowed is not None:
            ss = [jnp.where(allowed, s, NEG) for s in ss]
        top = m
        for s in ss:
            top = jnp.maximum(top, jnp.max(s, axis=0, keepdims=True))
        factor = jnp.exp2(m - top)
        l = ml[j, 1:2, :] * factor
        total = acc[j] * factor
        for s, (x, z) in zip(ss, blocks):
            p = jnp.exp2(s - top)
            l = l + jnp.sum(p, axis=0, keepdims=True)
            total = total + lax.dot_general(
                kv[x, z, 1], p.astype(bf16), (((1,), (0,)), ((), ())), preferred_element_type=f32
            )
        ml[j, 0:1, :] = top
        ml[j, 1:2, :] = l
        acc[j] = total

    if not last:
        krow = lax.broadcasted_iota(jnp.int32, (BLK, BLK), 0)
        qcol = lax.broadcasted_iota(jnp.int32, (BLK, BLK), 1)
        for j in range(4):
            step(j, [(xi, j)], krow <= qcol)

    def chunk(t, _):
        second = (t >= 1).astype(jnp.int32)
        third = (t >= 3).astype(jnp.int32)
        z = t - second - 2 * third
        step(1 + second + third, [(x, z) for x in range(4)])
        return 0

    lax.fori_loop(0, 6, chunk, 0)

    def pair(x, _):
        for j in range(4):
            step(j, [(x, j)])
        return 0

    lax.fori_loop(0, xi + core if last else xi, pair, 0)
    if last:
        for j in range(4):
            out[j] = (acc[j] / ml[j, 1:2, :]).astype(bf16)


def attend(where, kv, q, gate, state=None):
    hd = kv.shape[3]
    aug = hd + 16
    last = state is not None
    vmem = pl.BlockSpec(memory_space=pltpu.VMEM)
    smem = pl.BlockSpec(memory_space=pltpu.SMEM)
    held = [pltpu.VMEM((4, hd, BLK), f32), pltpu.VMEM((4, 8, BLK), f32)]
    carried = (jax.ShapeDtypeStruct((4, hd, BLK), f32), jax.ShapeDtypeStruct((4, 8, BLK), f32))
    return pl.pallas_call(
        functools.partial(attend_kernel, last=last),
        out_shape=jax.ShapeDtypeStruct((4, hd, BLK), bf16) if last else carried,
        in_specs=[smem, vmem, vmem, vmem] + ([vmem, vmem] if last else []),
        out_specs=vmem if last else (vmem, vmem),
        scratch_shapes=[pltpu.VMEM((4, 4, aug, BLK), bf16), pltpu.VMEM((4, aug, BLK), bf16)] + (held if last else []),
        cost_estimate=pl.CostEstimate(flops=2 * 10**9, bytes_accessed=2 * 10**6, transcendentals=10**6),
        name="attend_last" if last else "attend_first",
    )(where, kv, q, gate, *(state or ()))


def shards(
    hidden_in, w_convb, w_convc, w_convx, w_query, w_key, w_value, conv_taps, gate_cache, w_out_conv, w_out_attn
):
    zi = lax.axis_index("z")
    xi = lax.axis_index("x")
    ci = lax.axis_index("c")
    z_len = lax.axis_size("z")
    tok, width = hidden_in.shape
    rows, ch = w_convb.shape
    hd = w_query.shape[1] // 4
    per = hd + hd // 2
    half = ch // 2
    north = ci == 0
    place = (zi - 2) % 4
    cubes = [[(2 + 4 * g + i) % z_len for i in range(4)] for g in range(z_len // 4)]
    cubes_c = [[2 * z + c for z in cube for c in range(2)] for cube in cubes]
    swap = [(0, 1), (1, 0)]

    wq = w_query.reshape(rows, 4, hd)
    wk = w_key.reshape(rows, 4, hd)
    wv = w_value.reshape(rows, 4, hd)
    halves = []
    for c, w in enumerate((wk, wv)):
        heads = jnp.concatenate([w, wq[:, :, c * hd // 2 : (c + 1) * hd // 2]], axis=2).reshape(rows, 4 * per)
        convs = [w[:, c * half : (c + 1) * half] for w in (w_convb, w_convc, w_convx)]
        halves.append(jnp.concatenate([heads] + convs, axis=1))
    mine = jnp.where(north, halves[0], halves[1])
    theirs = lax.ppermute(jnp.where(north, halves[1], halves[0]), "c", swap)
    other = lax.ppermute(hidden_in, "c", swap)
    total = z_len * 8
    before = lax.ppermute(
        hidden_in[tok - 16 :], ("z", "x", "c"), [(i, (i + 1) % total) for i in range(total)]
    )
    w_rows = jnp.where(
        north, jnp.concatenate([mine, theirs], axis=0), jnp.concatenate([theirs, mine], axis=0)
    )
    w_all = lax.all_gather(w_rows, "z", axis=0, tiled=True)

    def over_x(w):
        w = lax.all_to_all(jnp.broadcast_to(w[None], (4,) + w.shape), "x", 0, 0, tiled=True)
        w = w.reshape(4, z_len, 2 * rows, w.shape[2]).transpose(1, 0, 2, 3)
        return w.reshape(width, w.shape[3])

    w_attn = over_x(w_all[:, : 4 * per])
    w_late, w_attn = lax.optimization_barrier((w_all[:, 4 * per :], w_attn))
    conv_mine = over_x(w_late)
    conv_theirs = lax.ppermute(conv_mine, "c", swap)

    tokens = jnp.concatenate([hidden_in, other], axis=0)
    proj = lax.dot_general(w_attn, tokens, (((0,), (1,)), ((), ())), preferred_element_type=f32)
    proj = proj.reshape(4, per, 2, tok)
    scale = jnp.where(jnp.arange(per) < hd, 1.0, LOG2E * hd**-0.5).astype(f32)
    proj = (proj * scale[None, :, None, None]).astype(bf16).transpose(0, 2, 1, 3)
    proj = jnp.where(north, proj, proj[:, ::-1]).reshape(8, per, tok)
    proj = lax.all_to_all(proj, ("z", "c"), 0, 0, tiled=True, axis_index_groups=cubes_c)
    proj = proj.reshape(4, 2, per, tok)
    q = proj[:, :, hd:].reshape(4, hd, tok)
    kv = proj[:, :, :hd]
    kv_own = lax.all_to_all(jnp.broadcast_to(kv[None], (4,) + kv.shape), "x", 0, 0, tiled=True)
    kv_own = kv_own.reshape(4, 4, 2, hd, tok)
    kv_oth = lax.ppermute(kv_own, "c", swap)

    gates = gate_cache.T
    stream = 32 * tok
    first = ((zi - place) % z_len) * 8 * tok
    low = lax.dynamic_slice(gates, (place, first), (1, stream // 2))
    high = lax.dynamic_slice(gates, (place, (first + stream // 2) % gates.shape[1]), (1, stream // 2))
    gate = jnp.concatenate([low, high], axis=1).reshape(32, tok)
    where = jnp.stack([ci, xi]).astype(jnp.int32)
    state = attend(where, kv_own, q, gate)
    heads = attend(where, kv_oth, q, gate, state)
    heads = lax.all_to_all(heads, "z", 0, 0, tiled=True, axis_index_groups=cubes)
    attn_out = heads.reshape(4 * hd, tok)

    longer = jnp.concatenate([before, hidden_in], axis=0)
    opening = (place == 0) & (xi == 0) & north
    keep = (jnp.arange(16 + tok)[:, None] >= 16) | jnp.logical_not(opening)

    def convolved(w, taps):
        trio = jnp.dot(longer, w, preferred_element_type=f32).astype(bf16).astype(f32)
        conv_input = (trio[:, half : 2 * half] * trio[:, 2 * half :]).astype(bf16).astype(f32)
        conv_input = jnp.where(keep, conv_input, 0.0)
        mixed_conv = (
            taps[0] * conv_input[14 : 14 + tok] + taps[1] * conv_input[15 : 15 + tok] + taps[2] * conv_input[16:]
        )
        return (trio[16:, :half] * mixed_conv).astype(bf16)

    taps0, taps1 = (conv_taps[:, :half], conv_taps[:, half:])
    conv_a = convolved(conv_mine, jnp.where(north, taps0, taps1))
    conv_b = convolved(conv_theirs, jnp.where(north, taps1, taps0))
    conv_out = jnp.where(
        north, jnp.concatenate([conv_a, conv_b], axis=1), jnp.concatenate([conv_b, conv_a], axis=1)
    )

    partial = jnp.dot(conv_out, w_out_conv, preferred_element_type=f32) + dot_t(attn_out, w_out_attn)
    partial = partial.astype(bf16).reshape(4, tok // 4, width)
    blocks = lax.all_to_all(partial, "y", 0, 0, tiled=True)
    return jnp.sum(blocks.astype(f32), axis=0).astype(bf16)


def solution(mesh):
    shape = mesh.devices.shape
    fine = Mesh(mesh.devices.reshape(shape[0] // 8, 4, 2, shape[1]), ("z", "x", "c", "y"))
    sp = ("z", "x", "c")
    return jax.shard_map(
        shards,
        mesh=fine,
        in_specs=(
            P(sp, None),
            P(sp, "y"),
            P(sp, "y"),
            P(sp, "y"),
            P(sp, "y"),
            P(sp, "y"),
            P(sp, "y"),
            P(None, "y"),
            P(None, "y"),
            P("y", None),
            P("y", None),
        ),
        out_specs=P(sp + ("y",), None),
        check_vma=False,
    )
```

time: 574 us -> 186 us (0.32)
  the two profiles are of different devices: /device:TPU:38 before, /device:TPU:6 now
where the time goes in v1:
time: 186 us; the launch traced here: 185 us
  blocking collectives  60.1 us (32%)
  starting transfers between devices  40.4 us (22%)
  waiting for transfers between devices  31.3 us (17%)
  Pallas kernels  22 us (12%)
  local copies, waits for them, and re-layouts  17.1 us (9%)
  matrix products  11 us (6%)
  other arithmetic  2.89 us (2%)
    all_gather x1, blocking collectives, shards(): w_all = lax.all_gather(w_rows, 'z', axis=0, tiled=True)  39.8 us
    pallas_call x2, Pallas kernels, attend(): pl.pallas_call(functools.partial(attend_kernel, last=last), out_shape=jax...  22 us
    all_to_all x1, blocking collectives, shards(): blocks = lax.all_to_all(partial, 'y', 0, 0, tiled=True)  20.3 us
    all_to_all x2, waiting for transfers between devices, over_x(): lax.all_to_all(jnp.broadcast_to(w[None], (4,) + w.shape), 'x', 0, 0, tile...  15.6 us
    all_to_all x1, waiting for transfers between devices, shards(): lax.all_to_all(jnp.broadcast_to(kv[None], (4,) + kv.shape), 'x', 0, 0, ti...  11 us
    all_to_all x2, starting transfers between devices, over_x(): lax.all_to_all(jnp.broadcast_to(w[None], (4,) + w.shape), 'x', 0, 0, tile...  10.4 us
    all_to_all x1, starting transfers between devices, shards(): lax.all_to_all(heads, 'z', 0, 0, tiled=True, axis_index_groups=cubes)  7.39 us
    all_to_all x1, starting transfers between devices, shards(): lax.all_to_all(proj, ('z', 'c'), 0, 0, tiled=True, axis_index_groups=cube...  5.41 us
  transfers between devices with their start and end apart: 10, of which 5 were waited for; matrix products, arithmetic and copies ran while one was open for 12% of the time, Pallas kernels for 6%

profile of v1, /device:TPU:6, one launch (start us, length us, event | category | flops | bytes accessed | tf_op | source)
XLA Modules:
  0.0 185.0 jit_solution(16987745541383807501)
XLA Ops:
  4.3 1.9 %collective-permute-start.1 = (bf16[16,768]{1,0:T(8,128)(2,1)S(1)}, bf16[16,768]{1,0:T(8,128)(2,1)S(1)}, u32[]{:S(2)}, u32[]{:S(2)}) collective-permute-start(bf16[16,768]{1,0:T(8,128)(2,1)S(1)} %get-tuple-element.18), channel_id=1, source_target_pairs={{0,4},{4,0},{1,5},{5,1},{2,6},{6,2},{3,7},{7,3},{8,12},{12,8},{9,1... | collective-permute-start | bytes 73736 | tf_op jit(solution)/shard_map/ppermute | solution.py:151
  7.4 39.8 %all_gather.3 = bf16[512,768]{1,0:T(8,128)(2,1)S(1)} all-gather(bf16[32,768]{1,0:T(8,128)(2,1)S(1)} %maximum_select_fusion.2), channel_id=1, replica_groups=mesh['z'=16,'x'=4,'c'=2,'y'=4] {'z'}, dimensions={0}, use_global_device_ids=true | all-gather | bytes 835584 | tf_op jit(solution)/shard_map/all_gather | solution.py:160
  48.5 4.8 %all-to-all-start = ((bf16[4,512,384]{2,1,0:T(8,128)(2,1)}), bf16[4,512,384]{2,1,0:T(8,128)(2,1)S(1)}, u32[]{:S(2)}, u32[]{:S(2)}) async-start(bf16[4,512,384]{2,1,0:T(8,128)(2,1)} %broadcast_in_dim.44), calls=%async_computation | async-start | bytes 3145728 | tf_op jit(solution)/shard_map/all_to_all | solution.py:163
  53.3 1.9 %collective-permute-start.3 = (bf16[256,2048]{1,0:T(8,128)(2,1)}, bf16[256,2048]{1,0:T(8,128)(2,1)}, u32[]{:S(2)}, u32[]{:S(2)}) collective-permute-start(bf16[256,2048]{1,0:T(8,128)(2,1)} %param.11), channel_id=1, source_target_pairs={{0,4},{4,0},{1,5},{5,1},{2,6},{6,2},{3,7},{7,3},{8,12},{12,8},{9,1... | collective-permute-start | bytes 3145736 | tf_op jit(solution)/shard_map/ppermute | solution.py:152
  55.2 10.4 %all-to-all-done = bf16[4,512,384]{2,1,0:T(8,128)(2,1)S(1)} async-done(((bf16[4,512,384]{2,1,0:T(8,128)(2,1)}), bf16[4,512,384]{2,1,0:T(8,128)(2,1)S(1)}, u32[]{:S(2)}, u32[]{:S(2)}) %all-to-all-start) | async-done | bytes 1572896 | tf_op jit(solution)/shard_map/all_to_all | solution.py:163
  68.3 5.6 %all-to-all-start.1 = ((bf16[4,512,384]{2,1,0:T(8,128)(2,1)}), bf16[4,512,384]{2,1,0:T(8,128)(2,1)S(1)}, u32[]{:S(2)}, u32[]{:S(2)}) async-start(bf16[4,512,384]{2,1,0:T(8,128)(2,1)} %broadcast_in_dim.45), calls=%async_computation.1 | async-start | bytes 3145728 | tf_op jit(solution)/shard_map/all_to_all | solution.py:163
  74.0 3.9 %fusion.1 = f32[384,512]{1,0:T(8,128)} fusion(bf16[2048,384]{1,0:T(8,128)(2,1)} %bitcast.44, bf16[256,2048]{1,0:T(8,128)(2,1)} %collective-permute-done.3, bf16[256,2048]{1,0:T(8,128)(2,1)} %param.11), kind=kOutput, calls=%fused_computation.2 | convolution fusion | flops 809500672 | bytes 4456448 | tf_op jit(solution)/shard_map/dot_general | solution.py:173
  77.9 1.6 reshape.74
  80.4 5.1 %all-to-all-done.1 = bf16[4,512,384]{2,1,0:T(8,128)(2,1)S(1)} async-done(((bf16[4,512,384]{2,1,0:T(8,128)(2,1)}), bf16[4,512,384]{2,1,0:T(8,128)(2,1)S(1)}, u32[]{:S(2)}, u32[]{:S(2)}) %all-to-all-start.1) | async-done | bytes 1572896 | tf_op jit(solution)/shard_map/all_to_all | solution.py:163
  85.6 5.4 %all-to-all-start.2 = ((bf16[8,96,256]{2,1,0:T(8,128)(2,1)}), bf16[8,96,256]{2,1,0:T(8,128)(2,1)S(1)}, u32[]{:S(2)}, u32[]{:S(2)}) async-start(bf16[8,96,256]{2,1,0:T(8,128)(2,1)} %bitcast.15), calls=%async_computation.2 | async-start | bytes 786432 | tf_op jit(solution)/shard_map/all_to_all | solution.py:178
  91.8 2.0 %collective-permute-start = (bf16[16,2048]{1,0:T(8,128)(2,1)S(1)}, bf16[16,2048]{1,0:T(8,128)(2,1)S(1)}, u32[]{:S(2)}, u32[]{:S(2)}) collective-permute-start(bf16[16,2048]{1,0:T(8,128)(2,1)S(1)} %slice.99), channel_id=1, source_target_pairs={{0,4},{4,8},{8,12},{12,16},{16,20},{20,24},{24,28},{28,32},{32,36}... | collective-permute-start | bytes 196616 | tf_op jit(solution)/shard_map/ppermute | solution.py:154
  95.0 1.4 copy.14
  96.4 4.9 %collective-permute-start.2 = (bf16[2048,384]{1,0:T(8,128)(2,1)}, bf16[2048,384]{1,0:T(8,128)(2,1)}, u32[]{:S(2)}, u32[]{:S(2)}) collective-permute-start(bf16[2048,384]{1,0:T(8,128)(2,1)} %bitcast.5), channel_id=1, source_target_pairs={{0,4},{4,0},{1,5},{5,1},{2,6},{6,2},{3,7},{7,3},{8,12},{12,8},{9,1... | collective-permute-start | bytes 4718600 | tf_op jit(solution)/shard_map/ppermute | solution.py:170
  103.1 4.6 %all-to-all-start.3 = ((bf16[4,4,2,64,256]{4,3,2,1,0:T(8,128)(2,1)}), bf16[4,4,2,64,256]{4,3,2,1,0:T(8,128)(2,1)}, u32[]{:S(2)}, u32[]{:S(2)}) async-start(bf16[4,4,2,64,256]{4,3,2,1,0:T(8,128)(2,1)} %broadcast_in_dim.50), calls=%async_computation.3 | async-start | bytes 2097152 | tf_op jit(solution)/shard_map/all_to_all | solution.py:182
  109.9 11.0 %all-to-all-done.3.kv = bf16[4,4,2,64,256]{4,3,2,1,0:T(8,128)(2,1)} async-done(((bf16[4,4,2,64,256]{4,3,2,1,0:T(8,128)(2,1)}), bf16[4,4,2,64,256]{4,3,2,1,0:T(8,128)(2,1)}, u32[]{:S(2)}, u32[]{:S(2)}) %all-to-all-start.3) | async-done | bytes 1048608 | tf_op jit(solution)/shard_map/all_to_all | solution.py:182
  120.9 1.9 %collective-permute-start.4 = (bf16[4,4,2,64,256]{4,3,2,1,0:T(8,128)(2,1)}, bf16[4,4,2,64,256]{4,3,2,1,0:T(8,128)(2,1)}, u32[]{:S(2)}, u32[]{:S(2)}) collective-permute-start(bf16[4,4,2,64,256]{4,3,2,1,0:T(8,128)(2,1)} %all-to-all-done.3.kv), channel_id=1, source_target_pairs={{0,4},{4,0},{1,5},{5,1},{2,6},{6,2},{3,7},{7,3},{8,12},{12,8},{9,1... | collective-permute-start | bytes 3145736 | tf_op jit(solution)/shard_map/ppermute | solution.py:184
  122.9 2.5 %fusion.6 = f32[272,384]{1,0:T(8,128)S(1)} fusion(bf16[272,2048]{1,0:T(8,128)(2,1)} %constant_dynamic-update-slice_fusion, bf16[2048,384]{1,0:T(8,128)(2,1)} %bitcast.5), kind=kOutput, calls=%fused_computation.9 | convolution fusion | flops 428027904 | bytes 3104768 | tf_op jit(solution)/shard_map/dot_general | solution.py:203
  126.0 11.6 %attend_first.1 = (f32[4,64,256]{2,1,0:T(8,128)}, f32[4,8,256]{2,1,0:T(8,128)}) custom-call(s32[2]{0:T(128)} %pad_add_fusion.where, bf16[4,4,2,64,256]{4,3,2,1,0:T(8,128)(2,1)} %all-to-all-done.3.kv, bf16[4,64,256]{2,1,0:T(8,128)(2,1)} %bitcast.48, f32[32,256]{1,0:T(8,128)} %reshape.78.gate), custom_call_target="tpu_custom_call" | custom-call | flops 2000000000 | bytes 2000000 | tf_op jit(solution)/shard_map/attend_first/pallas_call | solution.py:113
  137.6 2.5 %fusion.5 = f32[272,384]{1,0:T(8,128)S(1)} fusion(bf16[272,2048]{1,0:T(8,128)(2,1)} %constant_dynamic-update-slice_fusion, bf16[2048,384]{1,0:T(8,128)(2,1)} %collective-permute-done.2), kind=kOutput, calls=%fused_computation.7 | convolution fusion | flops 428027904 | bytes 3104768 | tf_op jit(solution)/shard_map/dot_general | solution.py:203
  140.3 10.4 %attend_last.1 = bf16[4,64,256]{2,1,0:T(8,128)(2,1)} custom-call(s32[2]{0:T(128)} %pad_add_fusion.where, bf16[4,4,2,64,256]{4,3,2,1,0:T(8,128)(2,1)} %collective-permute-done.4.kv, bf16[4,64,256]{2,1,0:T(8,128)(2,1)} %bitcast.49, f32[32,256]{1,0:T(8,128)} %reshape.78.gate, f32[4,64,256]{2,1,0:T(8,128)} %get-tuple-element.11.refs_0_, ...), custom_call_target="tpu_custom_call" | custom-call | flops 2000000000 | bytes 2000000 | tf_op jit(solution)/shard_map/attend_last/pallas_call | solution.py:113
  150.7 7.4 %all-to-all-start.4 = ((bf16[4,64,256]{2,1,0:T(8,128)(2,1)}), bf16[4,64,256]{2,1,0:T(8,128)(2,1)S(1)}, u32[]{:S(2)}, u32[]{:S(2)}) async-start(bf16[4,64,256]{2,1,0:T(8,128)(2,1)} %attend_last.1), calls=%async_computation.4 | async-start | bytes 262144 | tf_op jit(solution)/shard_map/all_to_all | solution.py:195
  158.6 3.5 %all-to-all-done.4 = bf16[4,64,256]{2,1,0:T(8,128)(2,1)S(1)} async-done(((bf16[4,64,256]{2,1,0:T(8,128)(2,1)}), bf16[4,64,256]{2,1,0:T(8,128)(2,1)S(1)}, u32[]{:S(2)}, u32[]{:S(2)}) %all-to-all-start.4) | async-done | bytes 131104 | tf_op jit(solution)/shard_map/all_to_all | solution.py:195
  162.1 1.7 fusion
  163.8 20.3 %all_to_all.30 = bf16[4,64,2048]{2,1,0:T(8,128)(2,1)S(1)} all-to-all(bf16[4,64,2048]{2,1,0:T(8,128)(2,1)S(1)} %bitcast.43), channel_id=1, replica_groups=mesh['z'=16,'x'=4,'c'=2,'y'=4] {'y'}, dimensions={0} | all-to-all | bytes 2097152 | tf_op jit(solution)/shard_map/all_to_all | solution.py:220
  (48 shorter events, 18.6 us)
Async XLA Ops:
  0.0 158.2 %copy-start = (bf16[256,2048]{1,0:T(8,128)(2,1)S(1)}, bf16[256,2048]{1,0:T(8,128)(2,1)}, u32[]{:S(2)}) copy-start(bf16[256,2048]{1,0:T(8,128)(2,1)} %param.20) | copy-start | bytes 3145732
  4.3 3.1 %collective-permute-start.1 = (bf16[16,768]{1,0:T(8,128)(2,1)S(1)}, bf16[16,768]{1,0:T(8,128)(2,1)S(1)}, u32[]{:S(2)}, u32[]{:S(2)}) collective-permute-start(bf16[16,768]{1,0:T(8,128)(2,1)S(1)} %get-tuple-element.18), channel_id=1, source_target_pairs={{0,4},{4,0},{1,5},{5,1},{2,6},{6,2},{3,7},{7,3},{8,12},{12,8},{9,1... | collective-permute-start | bytes 73736 | tf_op jit(solution)/shard_map/ppermute | solution.py:151
  48.5 17.1 %all-to-all-start = ((bf16[4,512,384]{2,1,0:T(8,128)(2,1)}), bf16[4,512,384]{2,1,0:T(8,128)(2,1)S(1)}, u32[]{:S(2)}, u32[]{:S(2)}) async-start(bf16[4,512,384]{2,1,0:T(8,128)(2,1)} %broadcast_in_dim.44), calls=%async_computation | async-start | bytes 3145728 | tf_op jit(solution)/shard_map/all_to_all | solution.py:163
  53.3 20.7 %collective-permute-start.3 = (bf16[256,2048]{1,0:T(8,128)(2,1)}, bf16[256,2048]{1,0:T(8,128)(2,1)}, u32[]{:S(2)}, u32[]{:S(2)}) collective-permute-start(bf16[256,2048]{1,0:T(8,128)(2,1)} %param.11), channel_id=1, source_target_pairs={{0,4},{4,0},{1,5},{5,1},{2,6},{6,2},{3,7},{7,3},{8,12},{12,8},{9,1... | collective-permute-start | bytes 3145736 | tf_op jit(solution)/shard_map/ppermute | solution.py:152
  68.3 17.2 %all-to-all-start.1 = ((bf16[4,512,384]{2,1,0:T(8,128)(2,1)}), bf16[4,512,384]{2,1,0:T(8,128)(2,1)S(1)}, u32[]{:S(2)}, u32[]{:S(2)}) async-start(bf16[4,512,384]{2,1,0:T(8,128)(2,1)} %broadcast_in_dim.45), calls=%async_computation.1 | async-start | bytes 3145728 | tf_op jit(solution)/shard_map/all_to_all | solution.py:163
  85.6 16.4 %all-to-all-start.2 = ((bf16[8,96,256]{2,1,0:T(8,128)(2,1)}), bf16[8,96,256]{2,1,0:T(8,128)(2,1)S(1)}, u32[]{:S(2)}, u32[]{:S(2)}) async-start(bf16[8,96,256]{2,1,0:T(8,128)(2,1)} %bitcast.15), calls=%async_computation.2 | async-start | bytes 786432 | tf_op jit(solution)/shard_map/all_to_all | solution.py:178
  91.8 16.5 %collective-permute-start = (bf16[16,2048]{1,0:T(8,128)(2,1)S(1)}, bf16[16,2048]{1,0:T(8,128)(2,1)S(1)}, u32[]{:S(2)}, u32[]{:S(2)}) collective-permute-start(bf16[16,2048]{1,0:T(8,128)(2,1)S(1)} %slice.99), channel_id=1, source_target_pairs={{0,4},{4,8},{8,12},{12,16},{16,20},{20,24},{24,28},{28,32},{32,36}... | collective-permute-start | bytes 196616 | tf_op jit(solution)/shard_map/ppermute | solution.py:154
  94.9 7.0 %copy-start.2 = (f32[3,256]{1,0:T(4,128)S(1)}, f32[3,256]{1,0:T(4,128)}, u32[]{:S(2)}) copy-start(f32[3,256]{1,0:T(4,128)} %param.18) | copy-start | bytes 9220
  96.4 41.3 %collective-permute-start.2 = (bf16[2048,384]{1,0:T(8,128)(2,1)}, bf16[2048,384]{1,0:T(8,128)(2,1)}, u32[]{:S(2)}, u32[]{:S(2)}) collective-permute-start(bf16[2048,384]{1,0:T(8,128)(2,1)} %bitcast.5), channel_id=1, source_target_pairs={{0,4},{4,0},{1,5},{5,1},{2,6},{6,2},{3,7},{7,3},{8,12},{12,8},{9,1... | collective-permute-start | bytes 4718600 | tf_op jit(solution)/shard_map/ppermute | solution.py:170
  102.0 6.9 %copy-start.1 = (bf16[256,2048]{1,0:T(8,128)(2,1)S(1)}, bf16[256,2048]{1,0:T(8,128)(2,1)}, u32[]{:S(2)}) copy-start(bf16[256,2048]{1,0:T(8,128)(2,1)} %param.11) | copy-start | bytes 3145732
  103.1 17.8 %all-to-all-start.3 = ((bf16[4,4,2,64,256]{4,3,2,1,0:T(8,128)(2,1)}), bf16[4,4,2,64,256]{4,3,2,1,0:T(8,128)(2,1)}, u32[]{:S(2)}, u32[]{:S(2)}) async-start(bf16[4,4,2,64,256]{4,3,2,1,0:T(8,128)(2,1)} %broadcast_in_dim.50), calls=%async_computation.3 | async-start | bytes 2097152 | tf_op jit(solution)/shard_map/all_to_all | solution.py:182
  120.9 19.4 %collective-permute-start.4 = (bf16[4,4,2,64,256]{4,3,2,1,0:T(8,128)(2,1)}, bf16[4,4,2,64,256]{4,3,2,1,0:T(8,128)(2,1)}, u32[]{:S(2)}, u32[]{:S(2)}) collective-permute-start(bf16[4,4,2,64,256]{4,3,2,1,0:T(8,128)(2,1)} %all-to-all-done.3.kv), channel_id=1, source_target_pairs={{0,4},{4,0},{1,5},{5,1},{2,6},{6,2},{3,7},{7,3},{8,12},{12,8},{9,1... | collective-permute-start | bytes 3145736 | tf_op jit(solution)/shard_map/ppermute | solution.py:184
  150.7 11.4 %all-to-all-start.4 = ((bf16[4,64,256]{2,1,0:T(8,128)(2,1)}), bf16[4,64,256]{2,1,0:T(8,128)(2,1)S(1)}, u32[]{:S(2)}, u32[]{:S(2)}) async-start(bf16[4,64,256]{2,1,0:T(8,128)(2,1)} %attend_last.1), calls=%async_computation.4 | async-start | bytes 262144 | tf_op jit(solution)/shard_map/all_to_all | solution.py:195

commit v2 on v1

v2 whole, which is shorter than its diff:
```python
import functools

import jax
import jax.numpy as jnp
from jax import lax
from jax.experimental import pallas as pl
from jax.experimental.pallas import tpu as pltpu
from jax.sharding import Mesh, PartitionSpec as P

LOG2E = 1.4426950408889634
NEG = -1e30
BLK = 256
bf16 = jnp.bfloat16
f32 = jnp.float32


def dot_t(a, b):
    return lax.dot_general(a, b, (((0,), (0,)), ((), ())), preferred_element_type=f32)


def dot(a, b):
    return lax.dot_general(a, b, (((1,), (0,)), ((), ())), preferred_element_type=f32)


def prepare_kernel(where, b, c, x, q, k, v, mine, theirs):
    core = where[0]
    heads = k.shape[1]
    half = heads // 2
    lane = lax.broadcasted_iota(jnp.int32, (heads, half), 0)
    col = lax.broadcasted_iota(jnp.int32, (heads, half), 1)

    def fill(out, side):
        pick = jnp.where(lane == (col // 32) * 64 + col % 32 + side * 32, 1.0, 0.0).astype(bf16)
        keep = jnp.broadcast_to(side, (k.shape[0], heads)) == 0
        out[:, 0:heads] = jnp.where(keep, k[...].astype(f32), v[...].astype(f32)).astype(bf16)
        out[:, heads : heads + half] = dot(q[...], pick).astype(bf16)
        at = heads + half
        for w in (b, c, x):
            both = jnp.where(keep[:, :half], w[:, :half].astype(f32), w[:, half:].astype(f32))
            out[:, at : at + half] = both.astype(bf16)
            at += half

    fill(mine, core)
    fill(theirs, 1 - core)


def prepare(where, *ws):
    rows, heads = ws[0].shape
    vmem = pl.BlockSpec(memory_space=pltpu.VMEM)
    shape = jax.ShapeDtypeStruct((rows, 3 * heads), bf16)
    return pl.pallas_call(
        prepare_kernel,
        out_shape=(shape, shape),
        in_specs=[pl.BlockSpec(memory_space=pltpu.SMEM)] + [vmem] * 6,
        out_specs=(vmem, vmem),
        name="prepare",
    )(where, *ws)


def ordered(w, wbuf):
    piece = w.shape[1] // 16
    for x in range(4):
        for z in range(16):
            at = (z * 4 + x) * piece
            wbuf[at : at + piece, :] = w[x, z * piece : (z + 1) * piece, :]


def project_kernel(where, w, own, oth, out, wbuf):
    core = where[0]
    hd = 64
    ordered(w, wbuf)
    for hidden, slot in ((own, core), (oth, 1 - core)):
        cols = dot(hidden[...], wbuf[...]).T
        for i in range(4):
            at = 4 * hd + i * hd // 2
            out[2 * i + slot, 0:hd, :] = cols[i * hd : (i + 1) * hd].astype(bf16)
            scaled = cols[at : at + hd // 2] * (LOG2E * hd**-0.5)
            out[2 * i + slot, hd : hd + hd // 2, :] = scaled.astype(bf16)


def project(where, w, own, oth):
    vmem = pl.BlockSpec(memory_space=pltpu.VMEM)
    return pl.pallas_call(
        project_kernel,
        out_shape=jax.ShapeDtypeStruct((8, 96, own.shape[0]), bf16),
        in_specs=[pl.BlockSpec(memory_space=pltpu.SMEM)] + [vmem] * 3,
        out_specs=vmem,
        scratch_shapes=[pltpu.VMEM((own.shape[1], w.shape[2]), bf16)],
        cost_estimate=pl.CostEstimate(flops=8 * 10**8, bytes_accessed=4 * 10**6, transcendentals=0),
        name="project",
    )(where, w, own, oth)


def convolve_kernel(where, w, hidden, before, taps, out, wbuf, line, *, swapped):
    tok = hidden.shape[0]
    lead = before.shape[0]
    half = out.shape[1]
    side = 1 - where[0] if swapped else where[0]
    ordered(w, wbuf)
    opening = where[2] == 1
    trio = dot(hidden[...], wbuf[...]).astype(bf16).astype(f32)
    edge = dot(before[...], wbuf[:, half:]).astype(bf16).astype(f32)
    first = (edge[:, :half] * edge[:, half:]).astype(bf16).astype(f32)
    line[0:lead, :] = jnp.where(jnp.broadcast_to(opening, first.shape), 0.0, first)
    line[lead : lead + tok, :] = (trio[:, half : 2 * half] * trio[:, 2 * half :]).astype(bf16).astype(f32)
    keep = jnp.broadcast_to(side, (3, half)) == 0
    tap = jnp.where(keep, taps[:, :half], taps[:, half:])
    mixed = (
        tap[0:1] * line[lead - 2 : lead - 2 + tok, :]
        + tap[1:2] * line[lead - 1 : lead - 1 + tok, :]
        + tap[2:3] * line[lead : lead + tok, :]
    )
    out[...] = (trio[:, :half] * mixed).astype(bf16)


def convolve(where, w, hidden, before, taps, swapped):
    vmem = pl.BlockSpec(memory_space=pltpu.VMEM)
    tok, width = hidden.shape
    half = taps.shape[1] // 2
    return pl.pallas_call(
        functools.partial(convolve_kernel, swapped=swapped),
        out_shape=jax.ShapeDtypeStruct((tok, half), bf16),
        in_specs=[pl.BlockSpec(memory_space=pltpu.SMEM)] + [vmem] * 4,
        out_specs=vmem,
        scratch_shapes=[
            pltpu.VMEM((width, w.shape[2]), bf16),
            pltpu.VMEM((tok + before.shape[0], half), f32),
        ],
        cost_estimate=pl.CostEstimate(flops=4 * 10**8, bytes_accessed=3 * 10**6, transcendentals=0),
        name="convolve_oth" if swapped else "convolve_own",
    )(where, w, hidden, before, taps)


def attend_kernel(where, kv, q, gate, *refs, last):
    if last:
        acc_in, ml_in, out, kbuf, qbuf, acc, ml = refs
    else:
        acc, ml, kbuf, qbuf = refs
    core = where[0]
    xi = where[1]
    hd = kv.shape[3]
    aug = qbuf.shape[1]
    cb = 1 - core if last else core

    if last:
        acc[...] = acc_in[...]
        ml[...] = ml_in[...]
    else:
        acc[...] = jnp.zeros_like(acc)
        line = lax.broadcasted_iota(jnp.int32, ml.shape, 1)
        ml[...] = jnp.where(line == 0, NEG, 0.0)

    row = lax.broadcasted_iota(jnp.int32, (aug - hd, BLK), 0)
    ones = jnp.where(row < 3, 1.0, 0.0).astype(bf16)
    for j in range(4):
        qbuf[j, 0:hd, :] = q[j]
        qbuf[j, hd:aug, :] = ones
    first = gate[0:1, 0:1]
    for z in range(4):
        for x in range(4):
            b = (first - gate[pl.ds(z * 8 + x * 2 + cb, 1), :]) * LOG2E
            hi = b.astype(bf16).astype(f32)
            rest = b - hi
            mid = rest.astype(bf16).astype(f32)
            lo = rest - mid
            rows = jnp.where(row == 0, hi, jnp.where(row == 1, mid, jnp.where(row == 2, lo, 0.0)))
            cols = jnp.concatenate([kv[x, z, 0].astype(f32), rows], axis=0)
            kbuf[x, z] = cols.T.astype(bf16)

    def steps(work, allowed=None):
        old = [(ml[j, 0:1, :], ml[j, 1:2, :], acc[j]) for j, _ in work]
        scores = []
        for j, blocks in work:
            qj = qbuf[j]
            ss = [dot(kbuf[x, z], qj) for x, z in blocks]
            scores.append(ss if allowed is None else [jnp.where(allowed, s, NEG) for s in ss])
        new = []
        for (j, blocks), ss, (m, l, total) in zip(work, scores, old):
            top = m
            for s in ss:
                top = jnp.maximum(top, jnp.max(s, axis=0, keepdims=True))
            factor = jnp.exp2(m - top)
            l = l * factor
            total = total * factor
            for s, (x, z) in zip(ss, blocks):
                p = jnp.exp2(s - top)
                l = l + jnp.sum(p, axis=0, keepdims=True)
                total = total + dot(kv[x, z, 1], p.astype(bf16))
            new.append((top, l, total))
        for (j, _), (top, l, total) in zip(work, new):
            ml[j, 0:1, :] = top
            ml[j, 1:2, :] = l
            acc[j] = total

    if not last:
        krow = lax.broadcasted_iota(jnp.int32, (BLK, BLK), 0)
        qcol = lax.broadcasted_iota(jnp.int32, (BLK, BLK), 1)
        steps([(j, [(xi, j)]) for j in range(4)], krow <= qcol)

    def chunk(t, _):
        second = (t >= 1).astype(jnp.int32)
        third = (t >= 3).astype(jnp.int32)
        z = t - second - 2 * third
        steps([(1 + second + third, [(x, z) for x in range(4)])])
        return 0

    lax.fori_loop(0, 6, chunk, 0)

    def pair(x, _):
        steps([(j, [(x, j)]) for j in range(4)])
        return 0

    lax.fori_loop(0, xi + core if last else xi, pair, 0)
    if last:
        for j in range(4):
            out[j] = (acc[j] / ml[j, 1:2, :]).astype(bf16)


def attend(where, kv, q, gate, state=None):
    hd = kv.shape[3]
    aug = 2 * hd
    last = state is not None
    vmem = pl.BlockSpec(memory_space=pltpu.VMEM)
    smem = pl.BlockSpec(memory_space=pltpu.SMEM)
    held = [pltpu.VMEM((4, hd, BLK), f32), pltpu.VMEM((4, 8, BLK), f32)]
    carried = (jax.ShapeDtypeStruct((4, hd, BLK), f32), jax.ShapeDtypeStruct((4, 8, BLK), f32))
    return pl.pallas_call(
        functools.partial(attend_kernel, last=last),
        out_shape=jax.ShapeDtypeStruct((4, hd, BLK), bf16) if last else carried,
        in_specs=[smem, vmem, vmem, vmem] + ([vmem, vmem] if last else []),
        out_specs=vmem if last else (vmem, vmem),
        scratch_shapes=[pltpu.VMEM((4, 4, BLK, aug), bf16), pltpu.VMEM((4, aug, BLK), bf16)] + (held if last else []),
        cost_estimate=pl.CostEstimate(flops=2 * 10**9, bytes_accessed=2 * 10**6, transcendentals=10**6),
        name="attend_last" if last else "attend_first",
    )(where, kv, q, gate, *(state or ()))


def shards(
    hidden_in, w_convb, w_convc, w_convx, w_query, w_key, w_value, conv_taps, gate_cache, w_out_conv, w_out_attn
):
    zi = lax.axis_index("z")
    xi = lax.axis_index("x")
    ci = lax.axis_index("c")
    z_len = lax.axis_size("z")
    tok, width = hidden_in.shape
    rows, ch = w_convb.shape
    hd = w_query.shape[1] // 4
    half = ch // 2
    north = ci == 0
    place = (zi - 2) % 4
    cubes = [[(2 + 4 * g + i) % z_len for i in range(4)] for g in range(z_len // 4)]
    cubes_c = [[2 * z + c for z in cube for c in range(2)] for cube in cubes]
    swap = [(0, 1), (1, 0)]
    opening = (place == 0) & (xi == 0) & north
    where = jnp.stack([ci, xi, opening.astype(jnp.int32)]).astype(jnp.int32)

    mine, theirs = prepare(where, w_convb, w_convc, w_convx, w_query, w_key, w_value)
    theirs = lax.ppermute(theirs, "c", swap)
    other = lax.ppermute(hidden_in, "c", swap)
    total = z_len * 8
    before = lax.ppermute(
        hidden_in[tok - 16 :], ("z", "x", "c"), [(i, (i + 1) % total) for i in range(total)]
    )
    w_rows = jnp.where(
        north, jnp.concatenate([mine, theirs], axis=0), jnp.concatenate([theirs, mine], axis=0)
    )
    w_all = lax.all_gather(w_rows, "z", axis=0, tiled=True)

    def over_x(w):
        return lax.all_to_all(jnp.broadcast_to(w[None], (4,) + w.shape), "x", 0, 0, tiled=True)

    w_attn = over_x(w_all[:, : ch + half])
    proj = project(where, w_attn, hidden_in, other)
    proj = lax.all_to_all(proj, ("z", "c"), 0, 0, tiled=True, axis_index_groups=cubes_c)
    proj = proj.reshape(4, 2, hd + hd // 2, tok)
    q = proj[:, :, hd:].reshape(4, hd, tok)
    kv = proj[:, :, :hd]
    kv_own = over_x(kv).reshape(4, 4, 2, hd, tok)
    w_late, kv_own = lax.optimization_barrier((w_all[:, ch + half :], kv_own))
    conv_mine = over_x(w_late)
    kv_oth = lax.ppermute(kv_own, "c", swap)

    gates = gate_cache.T
    stream = 32 * tok
    first = ((zi - place) % z_len) * 8 * tok
    low = lax.dynamic_slice(gates, (place, first), (1, stream // 2))
    high = lax.dynamic_slice(gates, (place, (first + stream // 2) % gates.shape[1]), (1, stream // 2))
    gate = jnp.concatenate([low, high], axis=1).reshape(32, tok)
    state = attend(where, kv_own, q, gate)
    heads = attend(where, kv_oth, q, gate, state)
    conv_mine, heads = lax.optimization_barrier((conv_mine, heads))
    heads = lax.all_to_all(heads, "z", 0, 0, tiled=True, axis_index_groups=cubes)
    attn_out = heads.reshape(4 * hd, tok)

    conv_theirs = lax.ppermute(conv_mine, "c", swap)
    conv_a = convolve(where, conv_mine, hidden_in, before, conv_taps, False)
    conv_b = convolve(where, conv_theirs, hidden_in, before, conv_taps, True)
    conv_out = jnp.where(
        north, jnp.concatenate([conv_a, conv_b], axis=1), jnp.concatenate([conv_b, conv_a], axis=1)
    )

    partial = jnp.dot(conv_out, w_out_conv, preferred_element_type=f32) + dot_t(attn_out, w_out_attn)
    partial = partial.astype(bf16).reshape(4, tok // 4, width)
    blocks = lax.all_to_all(partial, "y", 0, 0, tiled=True)
    return jnp.sum(blocks.astype(f32), axis=0).astype(bf16)


def solution(mesh):
    shape = mesh.devices.shape
    fine = Mesh(mesh.devices.reshape(shape[0] // 8, 4, 2, shape[1]), ("z", "x", "c", "y"))
    sp = ("z", "x", "c")
    return jax.shard_map(
        shards,
        mesh=fine,
        in_specs=(
            P(sp, None),
            P(sp, "y"),
            P(sp, "y"),
            P(sp, "y"),
            P(sp, "y"),
            P(sp, "y"),
            P(sp, "y"),
            P(None, "y"),
            P(None, "y"),
            P("y", None),
            P("y", None),
        ),
        out_specs=P(sp + ("y",), None),
        check_vma=False,
    )
```

time: 186 us -> 178 us (0.957)
  blocking collectives: 60.1 us -> 91.8 us
  waiting for transfers between devices: 31.3 us -> 15.9 us
  starting transfers between devices: 40.4 us -> 28.8 us
  local copies, waits for them, and re-layouts: 17.1 us -> 6.56 us
  matrix products: 11 us -> 2.2 us
  Pallas kernels: 22 us -> 29.7 us
    all_to_all x0 -> x2, blocking collectives: none -> 32.7 us  [the longest x1 17.7 us: over_x(): lax.all_to_all(jnp.broadcast_to(w[None], (4,) + w.shape), 'x', 0, 0, tile...]
    pallas_call x0 -> x4, Pallas kernels: none -> 12.2 us  [the longest x2 6.54 us: convolve(): pl.pallas_call(functools.partial(convolve_kernel, swapped=swapped), out_s...]
    all_to_all x2 -> x0, waiting for transfers between devices: 11 us -> none  [the longest x1 11 us: shards(): lax.all_to_all(jnp.broadcast_to(kv[None], (4,) + kv.shape), 'x', 0, 0, ti...]
    all_to_all x2 -> x0, starting transfers between devices: 9.97 us -> none  [the longest x1 5.41 us: shards(): lax.all_to_all(proj, ('z', 'c'), 0, 0, tiled=True, axis_index_groups=cube...]
    dot_general x3 -> x0, matrix products: 8.88 us -> none  [the longest x2 4.96 us: convolved(): jnp.dot(longer, w, preferred_element_type=f32).astype(bf16).astype(f32)]
    all_to_all x2, waiting for transfers between devices: 15.6 us -> 8.06 us  [over_x(): lax.all_to_all(jnp.broadcast_to(w[None], (4,) + w.shape), 'x', 0, 0, tile...]
    pallas_call x2, Pallas kernels: 22 us -> 17.5 us  [attend(): pl.pallas_call(functools.partial(attend_kernel, last=last), out_shape=jax...]
    reshape x6 -> x0, local copies, waits for them, and re-layouts: 4.23 us -> none  [the longest x1 1.62 us: shards(): proj = proj.reshape(4, per, 2, tok)]
  transfers between devices with their start and end apart: 10 -> 8, of which waited for: 5 -> 4; matrix products, arithmetic and copies ran while one was open for 12% -> 3% of each run, Pallas kernels for 6% -> 12%
where the time goes in v2:
time: 178 us; the launch traced here: 177 us
  blocking collectives  91.8 us (52%)
  Pallas kernels  29.7 us (17%)
  starting transfers between devices  28.8 us (16%)
  waiting for transfers between devices  15.9 us (9%)
  local copies, waits for them, and re-layouts  6.56 us (4%)
  other arithmetic  2.43 us (1%)
  matrix products  2.2 us (1%)
    all_gather x1, blocking collectives, shards(): w_all = lax.all_gather(w_rows, 'z', axis=0, tiled=True)  39.8 us
    all_to_all x1, blocking collectives, shards(): blocks = lax.all_to_all(partial, 'y', 0, 0, tiled=True)  19.3 us
    all_to_all x1, blocking collectives, over_x(): lax.all_to_all(jnp.broadcast_to(w[None], (4,) + w.shape), 'x', 0, 0, tile...  17.7 us
    pallas_call x2, Pallas kernels, attend(): pl.pallas_call(functools.partial(attend_kernel, last=last), out_shape=jax...  17.5 us
    all_to_all x1, blocking collectives, shards(): lax.all_to_all(proj, ('z', 'c'), 0, 0, tiled=True, axis_index_groups=cube...  15 us
    all_to_all x2, starting transfers between devices, over_x(): lax.all_to_all(jnp.broadcast_to(w[None], (4,) + w.shape), 'x', 0, 0, tile...  11.1 us
    all_to_all x2, waiting for transfers between devices, over_x(): lax.all_to_all(jnp.broadcast_to(w[None], (4,) + w.shape), 'x', 0, 0, tile...  8.06 us
    all_to_all x1, starting transfers between devices, shards(): lax.all_to_all(heads, 'z', 0, 0, tiled=True, axis_index_groups=cubes)  7.33 us
  transfers between devices with their start and end apart: 8, of which 4 were waited for; matrix products, arithmetic and copies ran while one was open for 3% of the time, Pallas kernels for 12%

profile of v2, /device:TPU:6, one launch (start us, length us, event | category | flops | bytes accessed | tf_op | source)
XLA Modules:
  0.0 177.4 jit_solution(5588494994438700731)
XLA Ops:
  0.6 1.6 prepare.1
  2.2 1.9 %collective-permute-start = (bf16[16,768]{1,0:T(8,128)(2,1)}, bf16[16,768]{1,0:T(8,128)(2,1)S(1)}, u32[]{:S(2)}, u32[]{:S(2)}) collective-permute-start(bf16[16,768]{1,0:T(8,128)(2,1)} %get-tuple-element.14), channel_id=1, source_target_pairs={{0,4},{4,0},{1,5},{5,1},{2,6},{6,2},{3,7},{7,3},{8,12},{12,8},{9,1... | collective-permute-start | bytes 73736 | tf_op jit(solution)/shard_map/ppermute | solution.py:258
  4.1 1.4 collective-permute-done
  6.3 39.8 %all_gather.3 = bf16[512,768]{1,0:T(8,128)(2,1)S(1)} all-gather(bf16[32,768]{1,0:T(8,128)(2,1)S(1)} %maximum_select_fusion.2), channel_id=1, replica_groups=mesh['z'=16,'x'=4,'c'=2,'y'=4] {'z'}, dimensions={0}, use_global_device_ids=true | all-gather | bytes 835584 | tf_op jit(solution)/shard_map/all_gather | solution.py:267
  46.2 1.3 broadcast_in_dim.6
  47.4 4.8 %all-to-all-start = ((bf16[4,512,384]{2,1,0:T(8,128)(2,1)}), bf16[4,512,384]{2,1,0:T(8,128)(2,1)}, u32[]{:S(2)}, u32[]{:S(2)}) async-start(bf16[4,512,384]{2,1,0:T(8,128)(2,1)} %broadcast_in_dim.6), calls=%async_computation | async-start | bytes 3145728 | tf_op jit(solution)/shard_map/all_to_all | solution.py:270
  52.2 1.9 %collective-permute-start.1 = (bf16[256,2048]{1,0:T(8,128)(2,1)S(1)}, bf16[256,2048]{1,0:T(8,128)(2,1)}, u32[]{:S(2)}, u32[]{:S(2)}) collective-permute-start(bf16[256,2048]{1,0:T(8,128)(2,1)S(1)} %copy-done.1), channel_id=1, source_target_pairs={{0,4},{4,0},{1,5},{5,1},{2,6},{6,2},{3,7},{7,3},{8,12},{12,8},{9,1... | collective-permute-start | bytes 3145736 | tf_op jit(solution)/shard_map/ppermute | solution.py:259
  54.1 2.8 %collective-permute-done.1.oth = bf16[256,2048]{1,0:T(8,128)(2,1)} collective-permute-done((bf16[256,2048]{1,0:T(8,128)(2,1)S(1)}, bf16[256,2048]{1,0:T(8,128)(2,1)}, u32[]{:S(2)}, u32[]{:S(2)}) %collective-permute-start.1) | collective-permute-done | bytes 1048608 | tf_op jit(solution)/shard_map/ppermute | solution.py:259
  56.9 8.1 %all-to-all-done.w = bf16[4,512,384]{2,1,0:T(8,128)(2,1)} async-done(((bf16[4,512,384]{2,1,0:T(8,128)(2,1)}), bf16[4,512,384]{2,1,0:T(8,128)(2,1)}, u32[]{:S(2)}, u32[]{:S(2)}) %all-to-all-start) | async-done | bytes 1572896 | tf_op jit(solution)/shard_map/all_to_all | solution.py:270
  65.0 4.1 %project.1 = bf16[8,96,256]{2,1,0:T(8,128)(2,1)} custom-call(s32[3]{0:T(128)} %pad_add_fusion.where, bf16[4,512,384]{2,1,0:T(8,128)(2,1)} %all-to-all-done.w, bf16[256,2048]{1,0:T(8,128)(2,1)} %hidden.3, bf16[256,2048]{1,0:T(8,128)(2,1)} %collective-permute-done.1.oth), custom_call_target="tpu_custom_call" | custom-call | flops 800000000 | bytes 4000000 | tf_op jit(solution)/shard_map/project/pallas_call | solution.py:83
  69.1 15.0 %all_to_all.30 = bf16[8,96,256]{2,1,0:T(8,128)(2,1)S(1)} all-to-all(bf16[8,96,256]{2,1,0:T(8,128)(2,1)} %project.1), channel_id=1, replica_groups={{64,68,96,100,128,132,160,164},{192,196,224,228,256,260,288,292},{320,3..., dimensions={0} | all-to-all | bytes 786432 | tf_op jit(solution)/shard_map/all_to_all | solution.py:274
  84.2 17.7 %all_to_all.31.kv = bf16[4,4,2,64,256]{4,3,2,1,0:T(8,128)(2,1)S(1)} all-to-all(bf16[4,4,2,64,256]{4,3,2,1,0:T(8,128)(2,1)S(1)} %broadcast_in_dim.7), channel_id=1, replica_groups=mesh['z'=16,'x'=4,'c'=2,'y'=4] {'x'}, dimensions={0} | all-to-all | bytes 2097152 | tf_op jit(solution)/shard_map/all_to_all | solution.py:270
  101.9 1.9 %collective-permute-start.2 = (bf16[4,4,2,64,256]{4,3,2,1,0:T(8,128)(2,1)S(1)}, bf16[4,4,2,64,256]{4,3,2,1,0:T(8,128)(2,1)}, u32[]{:S(2)}, u32[]{:S(2)}) collective-permute-start(bf16[4,4,2,64,256]{4,3,2,1,0:T(8,128)(2,1)S(1)} %all_to_all.31.kv), channel_id=1, source_target_pairs={{0,4},{4,0},{1,5},{5,1},{2,6},{6,2},{3,7},{7,3},{8,12},{12,8},{9,1... | collective-permute-start | bytes 3145736 | tf_op jit(solution)/shard_map/ppermute | solution.py:281
  105.1 6.4 %all-to-all-start.3 = ((bf16[4,512,384]{2,1,0:T(8,128)(2,1)}), bf16[4,512,384]{2,1,0:T(8,128)(2,1)}, u32[]{:S(2)}, u32[]{:S(2)}) async-start(bf16[4,512,384]{2,1,0:T(8,128)(2,1)} %broadcast_in_dim.8), calls=%async_computation.3 | async-start | bytes 3145728 | tf_op jit(solution)/shard_map/all_to_all | solution.py:270
  113.9 9.0 %attend_first.1 = (f32[4,64,256]{2,1,0:T(8,128)}, f32[4,8,256]{2,1,0:T(8,128)}) custom-call(s32[3]{0:T(128)} %pad_add_fusion.where, bf16[4,4,2,64,256]{4,3,2,1,0:T(8,128)(2,1)} %copy-done.2, bf16[4,64,256]{2,1,0:T(8,128)(2,1)} %bitcast.18, f32[32,256]{1,0:T(8,128)} %reshape.22.gate), custom_call_target="tpu_custom_call" | custom-call | flops 2000000000 | bytes 2000000 | tf_op jit(solution)/shard_map/attend_first/pallas_call | solution.py:227
  122.9 8.5 %attend_last.1 = bf16[4,64,256]{2,1,0:T(8,128)(2,1)} custom-call(s32[3]{0:T(128)} %pad_add_fusion.where, bf16[4,4,2,64,256]{4,3,2,1,0:T(8,128)(2,1)} %collective-permute-done.2.kv, bf16[4,64,256]{2,1,0:T(8,128)(2,1)} %bitcast.19, f32[32,256]{1,0:T(8,128)} %reshape.22.gate, f32[4,64,256]{2,1,0:T(8,128)} %get-tuple-element.17.refs_0_, ...), custom_call_target="tpu_custom_call" | custom-call | flops 2000000000 | bytes 2000000 | tf_op jit(solution)/shard_map/attend_last/pallas_call | solution.py:227
  131.4 2.7 %collective-permute-start.4 = (bf16[4,512,384]{2,1,0:T(8,128)(2,1)}, bf16[4,512,384]{2,1,0:T(8,128)(2,1)}, u32[]{:S(2)}, u32[]{:S(2)}) collective-permute-start(bf16[4,512,384]{2,1,0:T(8,128)(2,1)} %all-to-all-done.3.w), channel_id=1, source_target_pairs={{0,4},{4,0},{1,5},{5,1},{2,6},{6,2},{3,7},{7,3},{8,12},{12,8},{9,1... | collective-permute-start | bytes 4718600 | tf_op jit(solution)/shard_map/ppermute | solution.py:295
  134.0 7.3 %all-to-all-start.4 = ((bf16[4,64,256]{2,1,0:T(8,128)(2,1)}), bf16[4,64,256]{2,1,0:T(8,128)(2,1)S(1)}, u32[]{:S(2)}, u32[]{:S(2)}) async-start(bf16[4,64,256]{2,1,0:T(8,128)(2,1)} %attend_last.1), calls=%async_computation.4 | async-start | bytes 262144 | tf_op jit(solution)/shard_map/all_to_all | solution.py:292
  142.2 1.9 %collective-permute-start.3 = (bf16[16,2048]{1,0:T(8,128)(2,1)S(1)}, bf16[16,2048]{1,0:T(8,128)(2,1)S(1)}, u32[]{:S(2)}, u32[]{:S(2)}) collective-permute-start(bf16[16,2048]{1,0:T(8,128)(2,1)S(1)} %slice.19), channel_id=1, source_target_pairs={{0,4},{4,8},{8,12},{12,16},{16,20},{20,24},{24,28},{28,32},{32,36}... | collective-permute-start | bytes 196616 | tf_op jit(solution)/shard_map/ppermute | solution.py:261
  144.1 3.7 %collective-permute-done.3.before = bf16[16,2048]{1,0:T(8,128)(2,1)S(1)} collective-permute-done((bf16[16,2048]{1,0:T(8,128)(2,1)S(1)}, bf16[16,2048]{1,0:T(8,128)(2,1)S(1)}, u32[]{:S(2)}, u32[]{:S(2)}) %collective-permute-start.3) | collective-permute-done | bytes 65568 | tf_op jit(solution)/shard_map/ppermute | solution.py:261
  148.4 3.3 %convolve_own.1 = bf16[256,128]{1,0:T(8,128)(2,1)} custom-call(s32[3]{0:T(128)} %pad_add_fusion.where, bf16[4,512,384]{2,1,0:T(8,128)(2,1)} %all-to-all-done.3.w, bf16[256,2048]{1,0:T(8,128)(2,1)} %hidden.3, bf16[16,2048]{1,0:T(8,128)(2,1)} %copy-done.4, f32[3,256]{1,0:T(4,128)} %taps.3), custom_call_target="tpu_custom_call" | custom-call | flops 400000000 | bytes 3000000 | tf_op jit(solution)/shard_map/convolve_own/pallas_call | solution.py:120
  152.2 3.3 %convolve_oth.1 = bf16[256,128]{1,0:T(8,128)(2,1)} custom-call(s32[3]{0:T(128)} %pad_add_fusion.where, bf16[4,512,384]{2,1,0:T(8,128)(2,1)} %collective-permute-done.4.w, bf16[256,2048]{1,0:T(8,128)(2,1)} %hidden.3, bf16[16,2048]{1,0:T(8,128)(2,1)} %copy-done.4, f32[3,256]{1,0:T(4,128)} %taps.3), custom_call_target="tpu_custom_call" | custom-call | flops 400000000 | bytes 3000000 | tf_op jit(solution)/shard_map/convolve_oth/pallas_call | solution.py:120
  155.4 1.7 fusion
  157.2 19.3 %all_to_all.32 = bf16[4,64,2048]{2,1,0:T(8,128)(2,1)S(1)} all-to-all(bf16[4,64,2048]{2,1,0:T(8,128)(2,1)S(1)} %bitcast.14), channel_id=1, replica_groups=mesh['z'=16,'x'=4,'c'=2,'y'=4] {'y'}, dimensions={0} | all-to-all | bytes 2097152 | tf_op jit(solution)/shard_map/all_to_all | solution.py:304
  (27 shorter events, 8.2 us)
Async XLA Ops:
  0.0 151.7 %copy-start = (bf16[256,2048]{1,0:T(8,128)(2,1)S(1)}, bf16[256,2048]{1,0:T(8,128)(2,1)}, u32[]{:S(2)}) copy-start(bf16[256,2048]{1,0:T(8,128)(2,1)} %param.21) | copy-start | bytes 3145732
  2.2 3.3 %collective-permute-start = (bf16[16,768]{1,0:T(8,128)(2,1)}, bf16[16,768]{1,0:T(8,128)(2,1)S(1)}, u32[]{:S(2)}, u32[]{:S(2)}) collective-permute-start(bf16[16,768]{1,0:T(8,128)(2,1)} %get-tuple-element.14), channel_id=1, source_target_pairs={{0,4},{4,0},{1,5},{5,1},{2,6},{6,2},{3,7},{7,3},{8,12},{12,8},{9,1... | collective-permute-start | bytes 73736 | tf_op jit(solution)/shard_map/ppermute | solution.py:258
  46.1 6.1 %copy-start.1 = (bf16[256,2048]{1,0:T(8,128)(2,1)S(1)}, bf16[256,2048]{1,0:T(8,128)(2,1)}, u32[]{:S(2)}) copy-start(bf16[256,2048]{1,0:T(8,128)(2,1)} %hidden.3) | copy-start | bytes 3145732
  47.4 17.5 %all-to-all-start = ((bf16[4,512,384]{2,1,0:T(8,128)(2,1)}), bf16[4,512,384]{2,1,0:T(8,128)(2,1)}, u32[]{:S(2)}, u32[]{:S(2)}) async-start(bf16[4,512,384]{2,1,0:T(8,128)(2,1)} %broadcast_in_dim.6), calls=%async_computation | async-start | bytes 3145728 | tf_op jit(solution)/shard_map/all_to_all | solution.py:270
  52.2 4.7 %collective-permute-start.1 = (bf16[256,2048]{1,0:T(8,128)(2,1)S(1)}, bf16[256,2048]{1,0:T(8,128)(2,1)}, u32[]{:S(2)}, u32[]{:S(2)}) collective-permute-start(bf16[256,2048]{1,0:T(8,128)(2,1)S(1)} %copy-done.1), channel_id=1, source_target_pairs={{0,4},{4,0},{1,5},{5,1},{2,6},{6,2},{3,7},{7,3},{8,12},{12,8},{9,1... | collective-permute-start | bytes 3145736 | tf_op jit(solution)/shard_map/ppermute | solution.py:259
  101.9 3.2 %copy-start.2 = (bf16[4,4,2,64,256]{4,3,2,1,0:T(8,128)(2,1)}, bf16[4,4,2,64,256]{4,3,2,1,0:T(8,128)(2,1)S(1)}, u32[]{:S(2)}) copy-start(bf16[4,4,2,64,256]{4,3,2,1,0:T(8,128)(2,1)S(1)} %all_to_all.31.kv) | copy-start | bytes 3145732
  101.9 21.0 %collective-permute-start.2 = (bf16[4,4,2,64,256]{4,3,2,1,0:T(8,128)(2,1)S(1)}, bf16[4,4,2,64,256]{4,3,2,1,0:T(8,128)(2,1)}, u32[]{:S(2)}, u32[]{:S(2)}) collective-permute-start(bf16[4,4,2,64,256]{4,3,2,1,0:T(8,128)(2,1)S(1)} %all_to_all.31.kv), channel_id=1, source_target_pairs={{0,4},{4,0},{1,5},{5,1},{2,6},{6,2},{3,7},{7,3},{8,12},{12,8},{9,1... | collective-permute-start | bytes 3145736 | tf_op jit(solution)/shard_map/ppermute | solution.py:281
  105.1 26.3 %all-to-all-start.3 = ((bf16[4,512,384]{2,1,0:T(8,128)(2,1)}), bf16[4,512,384]{2,1,0:T(8,128)(2,1)}, u32[]{:S(2)}, u32[]{:S(2)}) async-start(bf16[4,512,384]{2,1,0:T(8,128)(2,1)} %broadcast_in_dim.8), calls=%async_computation.3 | async-start | bytes 3145728 | tf_op jit(solution)/shard_map/all_to_all | solution.py:270
  131.4 20.8 %collective-permute-start.4 = (bf16[4,512,384]{2,1,0:T(8,128)(2,1)}, bf16[4,512,384]{2,1,0:T(8,128)(2,1)}, u32[]{:S(2)}, u32[]{:S(2)}) collective-permute-start(bf16[4,512,384]{2,1,0:T(8,128)(2,1)} %all-to-all-done.3.w), channel_id=1, source_target_pairs={{0,4},{4,0},{1,5},{5,1},{2,6},{6,2},{3,7},{7,3},{8,12},{12,8},{9,1... | collective-permute-start | bytes 4718600 | tf_op jit(solution)/shard_map/ppermute | solution.py:295
  134.0 17.6 %all-to-all-start.4 = ((bf16[4,64,256]{2,1,0:T(8,128)(2,1)}), bf16[4,64,256]{2,1,0:T(8,128)(2,1)S(1)}, u32[]{:S(2)}, u32[]{:S(2)}) async-start(bf16[4,64,256]{2,1,0:T(8,128)(2,1)} %attend_last.1), calls=%async_computation.4 | async-start | bytes 262144 | tf_op jit(solution)/shard_map/all_to_all | solution.py:292
  142.2 5.6 %collective-permute-start.3 = (bf16[16,2048]{1,0:T(8,128)(2,1)S(1)}, bf16[16,2048]{1,0:T(8,128)(2,1)S(1)}, u32[]{:S(2)}, u32[]{:S(2)}) collective-permute-start(bf16[16,2048]{1,0:T(8,128)(2,1)S(1)} %slice.19), channel_id=1, source_target_pairs={{0,4},{4,8},{8,12},{12,16},{16,20},{20,24},{24,28},{28,32},{32,36}... | collective-permute-start | bytes 196616 | tf_op jit(solution)/shard_map/ppermute | solution.py:261
  147.8 0.6 copy-start.4
  152.1 3.3 %copy-start.3 = (bf16[256,128]{1,0:T(8,128)(2,1)S(1)}, bf16[256,128]{1,0:T(8,128)(2,1)}, u32[]{:S(2)}) copy-start(bf16[256,128]{1,0:T(8,128)(2,1)} %convolve_own.1) | copy-start | bytes 196612
